TPU v7x, 32 devices: a whole 2x2x4 slice. The times are simulated.
32 devices in a mesh: sp: 4 (over z), dp: 8 (over y, x, core).
Axes of the slice: x: 2, y: 2, z: 4, core: 2. Of those that a mesh axis runs over, the one named last changes fastest.
Arguments:
- inputs: bfloat16 [8, 544, 2048], P('dp', 'sp'), may hold values from -6 to 6
- query_vectors: bfloat16 [8, 544, 1024], P('dp', 'sp'), may hold values from -6 to 6
- key_vectors: bfloat16 [8, 544, 1024], P('dp', 'sp'), may hold values from -6 to 6
- value_vectors: bfloat16 [8, 544, 1024], P('dp', 'sp'), may hold values from -6 to 6
- cotangent: bfloat16 [8, 544, 1024], P('dp', 'sp'), may hold values from -6 to 6
- gate_prefix: float32 [8, 16, 544], P('dp', 'sp'), may hold values from -544 to 0, as said below
- value_weight: bfloat16 [2048, 1024], P('sp', 'dp'), may hold values from -0.125 to 0.125
Outputs:
- query_grad: bfloat16 [8, 544, 1024], P('dp', 'sp')
- key_grad: bfloat16 [8, 544, 1024], P('dp', 'sp')
- input_grad: bfloat16 [8, 544, 2048], P('dp', 'sp')
- weight_grad: float32 [2048, 1024], P('sp', 'dp')
Inputs may be any that keep to these rules, and one draw needn't show every extreme that they name: `gate_prefix`: non-increasing along the positions of each sequence and head.
All inputs are finite; a program needn't handle non-finite values.
Results may differ from a plain program's by a relative error of at most 0.015.
Values may be sent and summed in bfloat16 or wider, within the bound.
A program may use at most 128 MiB of HBM per device.

v0:
```python
import jax
import jax.numpy as jnp
from jax import lax
from jax.sharding import PartitionSpec as P

HEAD_DIM = 64


def attention_backward(query_heads, key_heads, value_heads, grad_heads, prefix):
    length = query_heads.shape[0]
    score_scale = HEAD_DIM ** (-0.5)
    block_count = max(1, length // 512)
    block_rows = length // block_count
    key_accum = jnp.zeros(key_heads.shape, jnp.float32)
    value_accum = jnp.zeros(key_heads.shape, jnp.float32)
    query_parts = []
    for block_index in range(block_count):
        first_row = block_index * block_rows
        last_row = first_row + block_rows
        query_rows = query_heads[first_row:last_row]
        key_rows = key_heads[:last_row]
        grad_rows = grad_heads[first_row:last_row]
        scores = (
            jnp.einsum("qhd,khd->hqk", query_rows, key_rows, preferred_element_type=jnp.float32)
            * score_scale
        )
        scores = scores + prefix[:, first_row:last_row, None] - prefix[:, None, :last_row]
        causal = jnp.arange(last_row)[None, :] <= (first_row + jnp.arange(block_rows))[:, None]
        scores = jnp.where(causal[None], scores, -jnp.inf)
        row_peak = jnp.max(scores, axis=-1, keepdims=True)
        raised_scores = jnp.exp(scores - row_peak)
        softmax_rows = raised_scores / jnp.sum(raised_scores, axis=-1, keepdims=True)
        softmax_low = softmax_rows.astype(jnp.bfloat16)
        value_accum = value_accum.at[:last_row].add(
            jnp.einsum("hqk,qhd->khd", softmax_low, grad_rows, preferred_element_type=jnp.float32)
        )
        softmax_grad = jnp.einsum(
            "qhd,khd->hqk", grad_rows, value_heads[:last_row], preferred_element_type=jnp.float32
        )
        row_term = jnp.sum(softmax_rows * softmax_grad, axis=-1, keepdims=True)
        score_low = (softmax_rows * (softmax_grad - row_term)).astype(jnp.bfloat16)
        query_parts.append(
            (
                jnp.einsum("hqk,khd->qhd", score_low, key_rows, preferred_element_type=jnp.float32)
                * score_scale
            ).astype(jnp.bfloat16)
        )
        key_accum = key_accum.at[:last_row].add(
            jnp.einsum("hqk,qhd->khd", score_low, query_rows, preferred_element_type=jnp.float32)
        )
    query_grad = jnp.concatenate(query_parts, axis=0)
    key_grad = (key_accum * score_scale).astype(jnp.bfloat16)
    return (query_grad, key_grad, value_accum.astype(jnp.bfloat16))


def shards(inputs, query_vectors, key_vectors, value_vectors, cotangent, gate_prefix, value_weight):
    query_seq, key_seq, value_seq, grad_seq, input_cols = (
        lax.all_to_all(query_vectors[0], "sp", split_axis=1, concat_axis=0, tiled=True),
        lax.all_to_all(key_vectors[0], "sp", split_axis=1, concat_axis=0, tiled=True),
        lax.all_to_all(value_vectors[0], "sp", split_axis=1, concat_axis=0, tiled=True),
        lax.all_to_all(cotangent[0], "sp", split_axis=1, concat_axis=0, tiled=True),
        lax.all_to_all(inputs[0], "sp", split_axis=1, concat_axis=0, tiled=True),
    )
    length = query_seq.shape[0]
    local_width = query_seq.shape[1]
    head_shape = (length, local_width // HEAD_DIM, HEAD_DIM)
    query_heads, key_heads, value_heads = attention_backward(
        query_seq.reshape(head_shape),
        key_seq.reshape(head_shape),
        value_seq.reshape(head_shape),
        grad_seq.reshape(head_shape),
        gate_prefix[0],
    )
    query_flat = query_heads.reshape(length, local_width)
    key_flat = key_heads.reshape(length, local_width)
    value_flat = value_heads.reshape(length, local_width)
    value_all = lax.all_gather(value_flat, "sp", axis=1, tiled=True)
    weight_block = lax.all_gather(value_weight, "dp", axis=1, tiled=True)
    weight_rows = lax.psum_scatter(
        lax.dot_general(
            value_all, input_cols, (((0,), (0,)), ((), ())), preferred_element_type=jnp.float32
        ).astype(jnp.bfloat16),
        "dp",
        scatter_dimension=0,
        tiled=True,
    ).astype(jnp.float32)
    weight_grad = weight_rows.T
    query_back, key_back = (
        lax.all_to_all(query_flat, "sp", split_axis=0, concat_axis=1, tiled=True),
        lax.all_to_all(key_flat, "sp", split_axis=0, concat_axis=1, tiled=True),
    )
    column_grad = lax.dot_general(
        value_all, weight_block, (((1,), (1,)), ((), ())), preferred_element_type=jnp.float32
    ).astype(jnp.bfloat16)
    input_grad = lax.all_to_all(column_grad, "sp", split_axis=0, concat_axis=1, tiled=True)
    return (query_back[None], key_back[None], input_grad[None], weight_grad)


def solution(mesh):
    in_specs = (
        P("dp", "sp", None),
        P("dp", "sp", None),
        P("dp", "sp", None),
        P("dp", "sp", None),
        P("dp", "sp", None),
        P("dp", "sp", None),
        P("sp", "dp"),
    )
    out_specs = (P("dp", "sp", None), P("dp", "sp", None), P("dp", "sp", None), P("sp", "dp"))
    return jax.shard_map(shards, mesh=mesh, in_specs=in_specs, out_specs=out_specs, check_vma=False)
```

profile of v0, /device:TPU:0, one launch (start us, length us, event | category | flops | bytes accessed | tf_op | source)
XLA Modules:
  0.0 171.9 jit_solution(9864498030525884451)
XLA Ops:
  9.1 6.3 %all-to-all-start = ((bf16[136,4,256]{2,0,1:T(8,128)(2,1)}), bf16[136,4,256]{2,0,1:T(8,128)(2,1)S(1)}, u32[]{:S(2)}, u32[]{:S(2)}) async-start(bf16[136,4,256]{2,0,1:T(8,128)(2,1)} %copy.61), calls=%async_computation | async-start | bytes 557056 | tf_op jit(solution)/shard_map/all_to_all | solution.py:58
  17.3 7.4 %all-to-all-done = bf16[136,4,256]{2,0,1:T(8,128)(2,1)S(1)} async-done(((bf16[136,4,256]{2,0,1:T(8,128)(2,1)}), bf16[136,4,256]{2,0,1:T(8,128)(2,1)S(1)}, u32[]{:S(2)}, u32[]{:S(2)}) %all-to-all-start) | async-done | bytes 278560 | tf_op jit(solution)/shard_map/all_to_all | solution.py:58
  24.7 3.5 %all-to-all-start.1 = ((bf16[136,4,256]{2,0,1:T(8,128)(2,1)}), bf16[136,4,256]{2,0,1:T(8,128)(2,1)S(1)}, u32[]{:S(2)}, u32[]{:S(2)}) async-start(bf16[136,4,256]{2,0,1:T(8,128)(2,1)} %copy.62), calls=%async_computation.1 | async-start | bytes 557056 | tf_op jit(solution)/shard_map/all_to_all | solution.py:59
  30.1 5.2 %all-to-all-done.1 = bf16[136,4,256]{2,0,1:T(8,128)(2,1)S(1)} async-done(((bf16[136,4,256]{2,0,1:T(8,128)(2,1)}), bf16[136,4,256]{2,0,1:T(8,128)(2,1)S(1)}, u32[]{:S(2)}, u32[]{:S(2)}) %all-to-all-start.1) | async-done | bytes 278560 | tf_op jit(solution)/shard_map/all_to_all | solution.py:59
  35.3 3.5 %all-to-all-start.2 = ((bf16[136,4,256]{2,0,1:T(8,128)(2,1)}), bf16[136,4,256]{2,0,1:T(8,128)(2,1)S(1)}, u32[]{:S(2)}, u32[]{:S(2)}) async-start(bf16[136,4,256]{2,0,1:T(8,128)(2,1)} %copy.65), calls=%async_computation.2 | async-start | bytes 557056 | tf_op jit(solution)/shard_map/all_to_all | solution.py:61
  40.2 5.4 %all-to-all-done.2 = bf16[136,4,256]{2,0,1:T(8,128)(2,1)S(1)} async-done(((bf16[136,4,256]{2,0,1:T(8,128)(2,1)}), bf16[136,4,256]{2,0,1:T(8,128)(2,1)S(1)}, u32[]{:S(2)}, u32[]{:S(2)}) %all-to-all-start.2) | async-done | bytes 278560 | tf_op jit(solution)/shard_map/all_to_all | solution.py:61
  46.3 4.4 %fusion.22 = (f32[4,544]{1,0:T(4,128)S(1)}, f32[4,544,544]{1,2,0:T(8,128)}) fusion(f32[4,544]{1,0:T(4,128)S(1)} %bitcast.46, pred[544,544]{0,1:T(8,128)(4,1)S(1)} %iota_compare_fusion, bf16[544,4,64]{0,2,1:T(8,128)(2,1)S(1)} %copy.63, bf16[544,4,64]{0,2,1:T(8,128)(2,1)S(1)} %copy.64), kind=kOutput, calls=%fused_computation.30 | convolution fusion | flops 158622240 | bytes 5605376 | tf_op jit(solution)/shard_map/sub | solution.py:31
  50.6 3.8 %fusion.11 = bf16[4,544,64]{1,2,0:T(8,128)(2,1)} fusion(bf16[544,4,64]{0,2,1:T(8,128)(2,1)S(1)} %copy.67, f32[4,544]{1,0:T(4,128)S(1)} %get-tuple-element.60, f32[4,544]{1,0:T(4,128)S(1)} %bitcast.47, pred[544,544]{0,1:T(8,128)(4,1)S(1)} %iota_compare_fusion, bf16[544,4,64]{0,2,1:T(8,128)(2,1)S(1)} %copy.63, bf16[544,4,64]{0,2,1:T(8,128)(2,1)S(1)} %copy.64), kind=kOutput, calls=%fused_computation.21 | convolution fusion | flops 311466656 | bytes 1427456 | tf_op jit(solution)/shard_map/hqk,qhd->khd/dot_general | solution.py:35
  55.4 3.5 %all-to-all-start.3 = ((bf16[136,4,256]{2,0,1:T(8,128)(2,1)}), bf16[136,4,256]{2,0,1:T(8,128)(2,1)S(1)}, u32[]{:S(2)}, u32[]{:S(2)}) async-start(bf16[136,4,256]{2,0,1:T(8,128)(2,1)} %copy.66), calls=%async_computation.3 | async-start | bytes 557056 | tf_op jit(solution)/shard_map/all_to_all | solution.py:60
  61.0 5.0 %all-to-all-done.3 = bf16[136,4,256]{2,0,1:T(8,128)(2,1)S(1)} async-done(((bf16[136,4,256]{2,0,1:T(8,128)(2,1)}), bf16[136,4,256]{2,0,1:T(8,128)(2,1)S(1)}, u32[]{:S(2)}, u32[]{:S(2)}) %all-to-all-start.3) | async-done | bytes 278560 | tf_op jit(solution)/shard_map/all_to_all | solution.py:60
  65.9 10.5 %all-to-all-start.7 = ((bf16[136,4,512]{2,0,1:T(8,128)(2,1)}), bf16[136,4,512]{2,0,1:T(8,128)(2,1)}, u32[]{:S(2)}, u32[]{:S(2)}) async-start(bf16[136,4,512]{2,0,1:T(8,128)(2,1)} %copy.80), calls=%async_computation.7 | async-start | bytes 1114112 | tf_op jit(solution)/shard_map/all_to_all | solution.py:62
  76.7 3.5 %multiply_reduce_fusion = (f32[4,544]{1,0:T(4,128)S(1)}, f32[4,544,544]{1,2,0:T(8,128)S(1)}) fusion(f32[4,544,544]{1,2,0:T(8,128)} %get-tuple-element.61, f32[4,544]{1,0:T(4,128)S(1)} %get-tuple-element.60, bf16[544,4,64]{0,2,1:T(8,128)(2,1)S(1)} %copy.67, bf16[544,4,64]{2,1,0:T(4,128)(2,1)S(1)} %reshape.151), kind=kOutput, calls=%fused_computation.2 | convolution fusion | flops 155068288 | bytes 10044416 | tf_op jit(solution)/shard_map/qhd,khd->hqk/dot_general | solution.py:37
  80.2 3.6 %multiply_convert_fusion = bf16[4,544,544]{1,2,0:T(8,128)(2,1)S(1)} fusion(f32[4,544,544]{1,2,0:T(8,128)S(1)} %get-tuple-element.63, f32[4,544]{1,0:T(4,128)S(1)} %get-tuple-element.62, f32[4,544,544]{1,2,0:T(8,128)} %get-tuple-element.61, f32[4,544]{1,0:T(4,128)S(1)} %get-tuple-element.60), kind=kLoop, calls=%fused_computation.1 | loop fusion | flops 4734976 | bytes 11854848 | tf_op jit(solution)/shard_map/convert_element_type | solution.py:41
  83.8 1.7 fusion.15
  85.5 1.3 reshape.153
  87.8 12.1 %all-to-all-done.7 = bf16[136,4,512]{2,0,1:T(8,128)(2,1)} async-done(((bf16[136,4,512]{2,0,1:T(8,128)(2,1)}), bf16[136,4,512]{2,0,1:T(8,128)(2,1)}, u32[]{:S(2)}, u32[]{:S(2)}) %all-to-all-start.7) | async-done | bytes 557088 | tf_op jit(solution)/shard_map/all_to_all | solution.py:62
  99.9 4.1 %all-to-all-start.5 = ((bf16[4,136,256]{2,1,0:T(8,128)(2,1)}), bf16[4,136,256]{2,1,0:T(8,128)(2,1)}, u32[]{:S(2)}, u32[]{:S(2)}) async-start(bf16[4,136,256]{2,1,0:T(8,128)(2,1)} %copy.86), calls=%async_computation.5 | async-start | bytes 557056 | tf_op jit(solution)/shard_map/all_to_all | solution.py:90
  104.3 3.4 %convolution_convert_fusion = bf16[1024,512]{1,0:T(8,128)(2,1)} fusion(bf16[544,1024]{0,1:T(8,128)(2,1)} %all-gather.3.cloned.1.call-done, bf16[544,512]{1,0:T(8,128)(2,1)} %bitcast.14), kind=kOutput, calls=%fused_computation.14 | convolution fusion | flops 570949632 | bytes 2719744 | tf_op jit(solution)/shard_map/dot_general | solution.py:80
  111.0 3.6 %all-to-all-start.4 = ((bf16[4,136,256]{2,1,0:T(8,128)(2,1)}), bf16[4,136,256]{2,1,0:T(8,128)(2,1)S(1)}, u32[]{:S(2)}, u32[]{:S(2)}) async-start(bf16[4,136,256]{2,1,0:T(8,128)(2,1)} %copy.85), calls=%async_computation.4 | async-start | bytes 557056 | tf_op jit(solution)/shard_map/all_to_all | solution.py:89
  114.6 9.8 %all-gather.5.cloned.1.call-done = bf16[512,1024]{1,0:T(8,128)(2,1)} async-done(((bf16[512,128]{1,0:T(8,128)(2,1)}), bf16[512,1024]{1,0:T(8,128)(2,1)}) %all-gather.5.cloned.1.call-update) | async-done | bytes 1048592 | tf_op jit(solution)/shard_map/all_gather | solution.py:78
  124.4 3.4 %convolution_convert_fusion.1 = bf16[544,512]{1,0:T(8,128)(2,1)} fusion(bf16[544,1024]{0,1:T(8,128)(2,1)} %all-gather.3.cloned.1.call-done, bf16[512,1024]{1,0:T(8,128)(2,1)} %all-gather.5.cloned.1.call-done), kind=kOutput, calls=%fused_computation.16 | convolution fusion | flops 570703872 | bytes 2719744 | tf_op jit(solution)/shard_map/dot_general | solution.py:92
  127.8 4.6 %all-to-all-start.6 = ((bf16[4,136,512]{2,1,0:T(8,128)(2,1)}), bf16[4,136,512]{2,1,0:T(8,128)(2,1)S(1)}, u32[]{:S(2)}, u32[]{:S(2)}) async-start(bf16[4,136,512]{2,1,0:T(8,128)(2,1)} %bitcast.11), calls=%async_computation.6 | async-start | bytes 1114112 | tf_op jit(solution)/shard_map/all_to_all | solution.py:95
  135.4 12.6 %all-to-all-done.6 = bf16[4,136,512]{2,1,0:T(8,128)(2,1)S(1)} async-done(((bf16[4,136,512]{2,1,0:T(8,128)(2,1)}), bf16[4,136,512]{2,1,0:T(8,128)(2,1)S(1)}, u32[]{:S(2)}, u32[]{:S(2)}) %all-to-all-start.6) | async-done | bytes 557088 | tf_op jit(solution)/shard_map/all_to_all | solution.py:95
  149.5 14.1 %reduce-scatter.2.cloned.1.call-done = bf16[128,512]{1,0:T(8,128)(2,1)} async-done(((bf16[1024,512]{1,0:T(8,128)(2,1)}), bf16[128,512]{1,0:T(8,128)(2,1)}) %reduce-scatter.2.cloned.1.call-update) | async-done | bytes 131088 | tf_op jit(solution)/shard_map/reduce_scatter | solution.py:79
  (49 shorter events, 21.7 us)
Async XLA Ops:
  7.2 39.1 %copy-start.4 = (f32[1,4,544]{2,1,0:T(4,128)S(1)}, f32[1,4,544]{2,1,0:T(4,128)}, u32[]{:S(2)}) copy-start(f32[1,4,544]{2,1,0:T(4,128)} %param.20) | copy-start | bytes 26116
  9.1 15.6 %all-to-all-start = ((bf16[136,4,256]{2,0,1:T(8,128)(2,1)}), bf16[136,4,256]{2,0,1:T(8,128)(2,1)S(1)}, u32[]{:S(2)}, u32[]{:S(2)}) async-start(bf16[136,4,256]{2,0,1:T(8,128)(2,1)} %copy.61), calls=%async_computation | async-start | bytes 557056 | tf_op jit(solution)/shard_map/all_to_all | solution.py:58
  24.7 10.6 %all-to-all-start.1 = ((bf16[136,4,256]{2,0,1:T(8,128)(2,1)}), bf16[136,4,256]{2,0,1:T(8,128)(2,1)S(1)}, u32[]{:S(2)}, u32[]{:S(2)}) async-start(bf16[136,4,256]{2,0,1:T(8,128)(2,1)} %copy.62), calls=%async_computation.1 | async-start | bytes 557056 | tf_op jit(solution)/shard_map/all_to_all | solution.py:59
  35.3 10.3 %all-to-all-start.2 = ((bf16[136,4,256]{2,0,1:T(8,128)(2,1)}), bf16[136,4,256]{2,0,1:T(8,128)(2,1)S(1)}, u32[]{:S(2)}, u32[]{:S(2)}) async-start(bf16[136,4,256]{2,0,1:T(8,128)(2,1)} %copy.65), calls=%async_computation.2 | async-start | bytes 557056 | tf_op jit(solution)/shard_map/all_to_all | solution.py:61
  38.7 65.5 %all-gather.3.cloned.1.call-start = ((), (), s32[]{:S(2)}) async-start(), calls=%async_computation.9 | async-start | bytes 1638400 | tf_op jit(solution)/shard_map/all_gather | solution.py:77
  40.2 10.5 %copy-start = (bf16[544,4,64]{0,2,1:T(8,128)(2,1)}, bf16[544,4,64]{0,2,1:T(8,128)(2,1)S(1)}, u32[]{:S(2)}) copy-start(bf16[544,4,64]{0,2,1:T(8,128)(2,1)S(1)} %copy.64) | copy-start | bytes 835588
  50.6 3.9 %copy-start.3 = (bf16[1,136,1024]{2,1,0:T(8,128)(2,1)S(1)}, bf16[1,136,1024]{2,1,0:T(8,128)(2,1)}, u32[]{:S(2)}) copy-start(bf16[1,136,1024]{2,1,0:T(8,128)(2,1)} %param.18) | copy-start | bytes 835588
  50.6 9.0 %copy-start.2 = (bf16[1,136,2048]{2,1,0:T(8,128)(2,1)S(1)}, bf16[1,136,2048]{2,1,0:T(8,128)(2,1)}, u32[]{:S(2)}) copy-start(bf16[1,136,2048]{2,1,0:T(8,128)(2,1)} %param.15) | copy-start | bytes 1671172
  55.4 10.5 %all-to-all-start.3 = ((bf16[136,4,256]{2,0,1:T(8,128)(2,1)}), bf16[136,4,256]{2,0,1:T(8,128)(2,1)S(1)}, u32[]{:S(2)}, u32[]{:S(2)}) async-start(bf16[136,4,256]{2,0,1:T(8,128)(2,1)} %copy.66), calls=%async_computation.3 | async-start | bytes 557056 | tf_op jit(solution)/shard_map/all_to_all | solution.py:60
  58.9 65.5 %all-gather.5.cloned.1.call-start = ((), (), s32[]{:S(2)}) async-start(), calls=%async_computation.10 | async-start | bytes 1179648 | tf_op jit(solution)/shard_map/all_gather | solution.py:78
  65.9 34.0 %all-to-all-start.7 = ((bf16[136,4,512]{2,0,1:T(8,128)(2,1)}), bf16[136,4,512]{2,0,1:T(8,128)(2,1)}, u32[]{:S(2)}, u32[]{:S(2)}) async-start(bf16[136,4,512]{2,0,1:T(8,128)(2,1)} %copy.80), calls=%async_computation.7 | async-start | bytes 1114112 | tf_op jit(solution)/shard_map/all_to_all | solution.py:62
  87.8 19.9 %copy-start.1 = (bf16[544,4,64]{0,2,1:T(8,128)(2,1)S(1)}, bf16[544,4,64]{0,2,1:T(8,128)(2,1)}, u32[]{:S(2)}) copy-start(bf16[544,4,64]{0,2,1:T(8,128)(2,1)} %copy-done) | copy-start | bytes 835588
  99.9 11.1 %all-to-all-start.5 = ((bf16[4,136,256]{2,1,0:T(8,128)(2,1)}), bf16[4,136,256]{2,1,0:T(8,128)(2,1)}, u32[]{:S(2)}, u32[]{:S(2)}) async-start(bf16[4,136,256]{2,1,0:T(8,128)(2,1)} %copy.86), calls=%async_computation.5 | async-start | bytes 557056 | tf_op jit(solution)/shard_map/all_to_all | solution.py:90
  104.0 59.6 %reduce-scatter.2.cloned.1.call-start = ((), (), s32[]{:S(2)}) async-start(), calls=%async_computation.11 | async-start | bytes 1179648 | tf_op jit(solution)/shard_map/reduce_scatter | solution.py:79
  111.0 16.8 %all-to-all-start.4 = ((bf16[4,136,256]{2,1,0:T(8,128)(2,1)}), bf16[4,136,256]{2,1,0:T(8,128)(2,1)S(1)}, u32[]{:S(2)}, u32[]{:S(2)}) async-start(bf16[4,136,256]{2,1,0:T(8,128)(2,1)} %copy.85), calls=%async_computation.4 | async-start | bytes 557056 | tf_op jit(solution)/shard_map/all_to_all | solution.py:89
  127.8 20.2 %all-to-all-start.6 = ((bf16[4,136,512]{2,1,0:T(8,128)(2,1)}), bf16[4,136,512]{2,1,0:T(8,128)(2,1)S(1)}, u32[]{:S(2)}, u32[]{:S(2)}) async-start(bf16[4,136,512]{2,1,0:T(8,128)(2,1)} %bitcast.11), calls=%async_computation.6 | async-start | bytes 1114112 | tf_op jit(solution)/shard_map/all_to_all | solution.py:95
Sparse Core Ops, SparseCore 0:
  54.6 45.5 all-gather.2
  102.0 22.3 all-gather.4
  127.6 35.9 reduce-scatter.1
where the time goes:
time: 173 us; the launch traced here: 172 us
  waiting for transfers between devices  73.5 us (42%)
  starting transfers between devices  39.8 us (23%)
  matrix products  20.9 us (12%)
  local copies, waits for them, and re-layouts  19.1 us (11%)
  between operations  14 us (8%)
  other arithmetic  4.58 us (3%)
    reduce_scatter x1, waiting for transfers between devices, shards(): lax.psum_scatter(lax.dot_general(value_all, input_cols, (((0,), (0,)), ((...  14.1 us
    all_to_all x1, waiting for transfers between devices, shards(): lax.all_to_all(column_grad, 'sp', split_axis=0, concat_axis=1, tiled=True)  12.6 us
    all_to_all x1, waiting for transfers between devices, shards(): lax.all_to_all(inputs[0], 'sp', split_axis=1, concat_axis=0, tiled=True)  12.1 us
    all_to_all x1, starting transfers between devices, shards(): lax.all_to_all(inputs[0], 'sp', split_axis=1, concat_axis=0, tiled=True)  10.5 us
    all_gather x1, waiting for transfers between devices, shards(): weight_block = lax.all_gather(value_weight, 'dp', axis=1, tiled=True)  9.81 us
    all_to_all x1, waiting for transfers between devices, shards(): lax.all_to_all(query_vectors[0], 'sp', split_axis=1, concat_axis=0, tiled...  7.36 us
    all_to_all x1, starting transfers between devices, shards(): lax.all_to_all(query_vectors[0], 'sp', split_axis=1, concat_axis=0, tiled...  6.35 us
    all_to_all x1, waiting for transfers between devices, shards(): lax.all_to_all(cotangent[0], 'sp', split_axis=1, concat_axis=0, tiled=True)  5.43 us
  transfers between devices with their start and end apart: 11, of which 9 were waited for; matrix products, arithmetic and copies ran while one was open for 17% of the time, Pallas kernels for 0%

commit v1 on v0

--- a/solution.py
+++ b/solution.py
@@ -1,9 +1,32 @@
+import functools
 import jax
 import jax.numpy as jnp
 from jax import lax
 from jax.sharding import PartitionSpec as P
 
 HEAD_DIM = 64
+
+
+def turn_the_table(own_rows, mesh_dim):
+    sides = lax.axis_size(mesh_dim)
+    block_next = map(lambda j: (j, (j + 1) % sides), range(sides))
+    so_far_all = list(block_next)
+
+    def _perform_series_all(all_values):
+        if len(all_values) == sides:
+            return all_values
+        return _perform_series_all(
+            [lax.ppermute(all_values[0], axis_name=mesh_dim, perm=so_far_all), *all_values]
+        )
+
+    return jnp.roll(
+        jnp.concatenate(_perform_series_all([own_rows]), axis=1),
+        (lax.axis_index(mesh_dim) + 1) * own_rows.shape[1],
+        axis=1,
+    )
+
+
+open_sheet = functools.partial(turn_the_table, mesh_dim="dp")
 
 
 def attention_backward(query_heads, key_heads, value_heads, grad_heads, prefix):
@@ -75,7 +98,7 @@
     key_flat = key_heads.reshape(length, local_width)
     value_flat = value_heads.reshape(length, local_width)
     value_all = lax.all_gather(value_flat, "sp", axis=1, tiled=True)
-    weight_block = lax.all_gather(value_weight, "dp", axis=1, tiled=True)
+    weight_block = open_sheet(value_weight)
     weight_rows = lax.psum_scatter(
         lax.dot_general(
             value_all, input_cols, (((0,), (0,)), ((), ())), preferred_element_type=jnp.float32

time: 173 us -> 164 us (0.948)
  local copies, waits for them, and re-layouts: 19.1 us -> 28.4 us
  waiting for transfers between devices: 73.5 us -> 64.4 us
  starting transfers between devices: 39.8 us -> 33.9 us
  other arithmetic: 4.58 us -> 1.92 us
    ppermute x0 -> x7, waiting for transfers between devices: none -> 24.4 us  [_perform_series_all(): lax.ppermute(all_values[0], axis_name=mesh_dim, perm=so_far_all)]
    all_to_all x1, waiting for transfers between devices: 12.1 us -> 0.01 us  [shards(): lax.all_to_all(inputs[0], 'sp', split_axis=1, concat_axis=0, tiled=True)]
    reduce_scatter x1, waiting for transfers between devices: 14.1 us -> 3.18 us  [shards(): lax.psum_scatter(lax.dot_general(value_all, input_cols, (((0,), (0,)), ((...]
    unnamed x11 -> x34, local copies, waits for them, and re-layouts: 0.86 us -> 11.6 us
    all_gather x1 -> x0, waiting for transfers between devices: 9.81 us -> none  [shards(): weight_block = lax.all_gather(value_weight, 'dp', axis=1, tiled=True)]
    all_to_all x1, starting transfers between devices: 10.5 us -> 5.05 us  [shards(): lax.all_to_all(inputs[0], 'sp', split_axis=1, concat_axis=0, tiled=True)]
    all_to_all x1, waiting for transfers between devices: 4.95 us -> 0.01 us  [shards(): lax.all_to_all(value_vectors[0], 'sp', split_axis=1, concat_axis=0, tiled...]
    all_to_all x1, starting transfers between devices: 6.35 us -> 3.45 us  [shards(): lax.all_to_all(query_vectors[0], 'sp', split_axis=1, concat_axis=0, tiled...]
  transfers between devices with their start and end apart: 11 -> 17, of which waited for: 9 -> 13; matrix products, arithmetic and copies ran while one was open for 17% -> 27% of each run, Pallas kernels for 0% -> 0%
where the time goes in v1:
time: 164 us; the launch traced here: 163 us
  waiting for transfers between devices  64.4 us (39%)
  starting transfers between devices  33.9 us (21%)
  local copies, waits for them, and re-layouts  28.4 us (17%)
  matrix products  19.7 us (12%)
  between operations  14.3 us (9%)
  other arithmetic  1.92 us (1%)
    ppermute x7, waiting for transfers between devices, _perform_series_all(): lax.ppermute(all_values[0], axis_name=mesh_dim, perm=so_far_all)  24.4 us
    unnamed x34, local copies, waits for them, and re-layouts  11.6 us
    all_to_all x1, waiting for transfers between devices, shards(): lax.all_to_all(column_grad, 'sp', split_axis=0, concat_axis=1, tiled=True)  11 us
    all_to_all x1, waiting for transfers between devices, shards(): lax.all_to_all(key_vectors[0], 'sp', split_axis=1, concat_axis=0, tiled=T...  7.35 us
    all_to_all x1, starting transfers between devices, shards(): lax.all_to_all(key_vectors[0], 'sp', split_axis=1, concat_axis=0, tiled=T...  6.35 us
    all_to_all x1, waiting for transfers between devices, shards(): lax.all_to_all(query_vectors[0], 'sp', split_axis=1, concat_axis=0, tiled...  6.18 us
    all_to_all x1, waiting for transfers between devices, shards(): lax.all_to_all(cotangent[0], 'sp', split_axis=1, concat_axis=0, tiled=True)  5.93 us
    all_to_all x1, starting transfers between devices, shards(): lax.all_to_all(query_flat, 'sp', split_axis=0, concat_axis=1, tiled=True)  5.09 us
  transfers between devices with their start and end apart: 17, of which 13 were waited for; matrix products, arithmetic and copies ran while one was open for 27% of the time, Pallas kernels for 0%

profile of v1, /device:TPU:0, one launch (start us, length us, event | category | flops | bytes accessed | tf_op | source)
XLA Modules:
  0.0 162.7 jit_solution(5597326827481229056)
XLA Ops:
  9.1 6.3 %all-to-all-start.1 = ((bf16[136,4,256]{2,0,1:T(8,128)(2,1)}), bf16[136,4,256]{2,0,1:T(8,128)(2,1)S(1)}, u32[]{:S(2)}, u32[]{:S(2)}) async-start(bf16[136,4,256]{2,0,1:T(8,128)(2,1)} %copy.62), calls=%async_computation.1 | async-start | bytes 557056 | tf_op jit(solution)/shard_map/all_to_all | solution.py:82
  17.4 7.3 %all-to-all-done.1 = bf16[136,4,256]{2,0,1:T(8,128)(2,1)S(1)} async-done(((bf16[136,4,256]{2,0,1:T(8,128)(2,1)}), bf16[136,4,256]{2,0,1:T(8,128)(2,1)S(1)}, u32[]{:S(2)}, u32[]{:S(2)}) %all-to-all-start.1) | async-done | bytes 278560 | tf_op jit(solution)/shard_map/all_to_all | solution.py:82
  24.7 3.5 %all-to-all-start = ((bf16[136,4,256]{2,0,1:T(8,128)(2,1)}), bf16[136,4,256]{2,0,1:T(8,128)(2,1)S(1)}, u32[]{:S(2)}, u32[]{:S(2)}) async-start(bf16[136,4,256]{2,0,1:T(8,128)(2,1)} %copy.61), calls=%async_computation | async-start | bytes 557056 | tf_op jit(solution)/shard_map/all_to_all | solution.py:81
  29.1 6.2 %all-to-all-done = bf16[136,4,256]{2,0,1:T(8,128)(2,1)S(1)} async-done(((bf16[136,4,256]{2,0,1:T(8,128)(2,1)}), bf16[136,4,256]{2,0,1:T(8,128)(2,1)S(1)}, u32[]{:S(2)}, u32[]{:S(2)}) %all-to-all-start) | async-done | bytes 278560 | tf_op jit(solution)/shard_map/all_to_all | solution.py:81
  35.3 3.5 %all-to-all-start.2 = ((bf16[136,4,256]{2,0,1:T(8,128)(2,1)}), bf16[136,4,256]{2,0,1:T(8,128)(2,1)S(1)}, u32[]{:S(2)}, u32[]{:S(2)}) async-start(bf16[136,4,256]{2,0,1:T(8,128)(2,1)} %copy.65), calls=%async_computation.2 | async-start | bytes 557056 | tf_op jit(solution)/shard_map/all_to_all | solution.py:84
  39.7 5.9 %all-to-all-done.2 = bf16[136,4,256]{2,0,1:T(8,128)(2,1)S(1)} async-done(((bf16[136,4,256]{2,0,1:T(8,128)(2,1)}), bf16[136,4,256]{2,0,1:T(8,128)(2,1)S(1)}, u32[]{:S(2)}, u32[]{:S(2)}) %all-to-all-start.2) | async-done | bytes 278560 | tf_op jit(solution)/shard_map/all_to_all | solution.py:84
  45.7 3.5 %all-to-all-start.3 = ((bf16[136,4,256]{2,0,1:T(8,128)(2,1)}), bf16[136,4,256]{2,0,1:T(8,128)(2,1)S(1)}, u32[]{:S(2)}, u32[]{:S(2)}) async-start(bf16[136,4,256]{2,0,1:T(8,128)(2,1)} %copy.66), calls=%async_computation.3 | async-start | bytes 557056 | tf_op jit(solution)/shard_map/all_to_all | solution.py:83
  49.2 5.3 %collective-permute-done = bf16[512,128]{1,0:T(8,128)(2,1)S(1)} collective-permute-done((bf16[512,128]{1,0:T(8,128)(2,1)S(1)}, bf16[512,128]{1,0:T(8,128)(2,1)S(1)}, u32[]{:S(2)}, u32[]{:S(2)}) %collective-permute-start) | collective-permute-done | bytes 131104 | tf_op jit(solution)/shard_map/ppermute | solution.py:19
  54.5 5.3 %collective-permute-done.1 = bf16[512,128]{1,0:T(8,128)(2,1)S(1)} collective-permute-done((bf16[512,128]{1,0:T(8,128)(2,1)S(1)}, bf16[512,128]{1,0:T(8,128)(2,1)S(1)}, u32[]{:S(2)}, u32[]{:S(2)}) %collective-permute-start.1) | collective-permute-done | bytes 131104 | tf_op jit(solution)/shard_map/ppermute | solution.py:19
  61.2 3.9 %collective-permute-done.2 = bf16[512,128]{1,0:T(8,128)(2,1)S(1)} collective-permute-done((bf16[512,128]{1,0:T(8,128)(2,1)S(1)}, bf16[512,128]{1,0:T(8,128)(2,1)S(1)}, u32[]{:S(2)}, u32[]{:S(2)}) %collective-permute-start.2) | collective-permute-done | bytes 131104 | tf_op jit(solution)/shard_map/ppermute | solution.py:19
  67.7 5.0 %all-to-all-start.7 = ((bf16[136,4,512]{2,0,1:T(8,128)(2,1)}), bf16[136,4,512]{2,0,1:T(8,128)(2,1)S(1)}, u32[]{:S(2)}, u32[]{:S(2)}) async-start(bf16[136,4,512]{2,0,1:T(8,128)(2,1)} %copy.80), calls=%async_computation.7 | async-start | bytes 1114112 | tf_op jit(solution)/shard_map/all_to_all | solution.py:85
  73.0 4.3 %fusion.24 = (f32[4,544]{1,0:T(4,128)S(1)}, f32[4,544,544]{1,2,0:T(8,128)}) fusion(f32[4,544]{1,0:T(4,128)S(1)} %bitcast.49, pred[544,544]{0,1:T(8,128)(4,1)S(1)} %iota_compare_fusion, bf16[544,4,64]{0,2,1:T(8,128)(2,1)S(1)} %copy.63, bf16[544,4,64]{0,2,1:T(8,128)(2,1)S(1)} %copy.64), kind=kOutput, calls=%fused_computation.48 | convolution fusion | flops 158622240 | bytes 5605376 | tf_op jit(solution)/shard_map/sub | solution.py:54
  77.3 3.8 %fusion.11 = bf16[4,544,64]{1,2,0:T(8,128)(2,1)} fusion(bf16[544,4,64]{0,2,1:T(8,128)(2,1)S(1)} %copy-done.2, f32[4,544]{1,0:T(4,128)S(1)} %get-tuple-element.60, f32[4,544]{1,0:T(4,128)S(1)} %bitcast.50, pred[544,544]{0,1:T(8,128)(4,1)S(1)} %iota_compare_fusion, bf16[544,4,64]{0,2,1:T(8,128)(2,1)S(1)} %copy.63, bf16[544,4,64]{0,2,1:T(8,128)(2,1)S(1)} %copy.64), kind=kOutput, calls=%fused_computation.21 | convolution fusion | flops 311466656 | bytes 1427456 | tf_op jit(solution)/shard_map/hqk,qhd->khd/dot_general | solution.py:58
  81.2 3.6 %multiply_reduce_fusion = (f32[4,544]{1,0:T(4,128)S(1)}, f32[4,544,544]{1,2,0:T(8,128)S(1)}) fusion(f32[4,544,544]{1,2,0:T(8,128)} %get-tuple-element.61, f32[4,544]{1,0:T(4,128)S(1)} %get-tuple-element.60, bf16[544,4,64]{0,2,1:T(8,128)(2,1)S(1)} %copy-done.2, bf16[544,4,64]{2,1,0:T(4,128)(2,1)S(1)} %reshape.151), kind=kOutput, calls=%fused_computation.2 | convolution fusion | flops 155068288 | bytes 10044416 | tf_op jit(solution)/shard_map/qhd,khd->hqk/dot_general | solution.py:60
  86.3 3.9 %collective-permute-done.4 = bf16[512,128]{1,0:T(8,128)(2,1)S(1)} collective-permute-done((bf16[512,128]{1,0:T(8,128)(2,1)S(1)}, bf16[512,128]{1,0:T(8,128)(2,1)S(1)}, u32[]{:S(2)}, u32[]{:S(2)}) %collective-permute-start.4) | collective-permute-done | bytes 131104 | tf_op jit(solution)/shard_map/ppermute | solution.py:19
  90.8 4.6 %collective-permute-done.5 = bf16[512,128]{1,0:T(8,128)(2,1)S(1)} collective-permute-done((bf16[512,128]{1,0:T(8,128)(2,1)S(1)}, bf16[512,128]{1,0:T(8,128)(2,1)S(1)}, u32[]{:S(2)}, u32[]{:S(2)}) %collective-permute-start.5) | collective-permute-done | bytes 131104 | tf_op jit(solution)/shard_map/ppermute | solution.py:19
  108.3 5.1 %all-to-all-start.4 = ((bf16[4,136,256]{2,1,0:T(8,128)(2,1)}), bf16[4,136,256]{2,1,0:T(8,128)(2,1)S(1)}, u32[]{:S(2)}, u32[]{:S(2)}) async-start(bf16[4,136,256]{2,1,0:T(8,128)(2,1)} %copy.85), calls=%async_computation.4 | async-start | bytes 557056 | tf_op jit(solution)/shard_map/all_to_all | solution.py:112
  116.2 3.3 %convolution_convert_fusion = bf16[1024,512]{1,0:T(8,128)(2,1)} fusion(bf16[544,1024]{0,1:T(8,128)(2,1)} %all-gather.2.cloned.1.call-done, bf16[544,512]{1,0:T(8,128)(2,1)S(1)} %bitcast.47), kind=kOutput, calls=%fused_computation.14 | convolution fusion | flops 570949632 | bytes 2719744 | tf_op jit(solution)/shard_map/dot_general | solution.py:103
  121.5 3.5 %all-to-all-start.5 = ((bf16[4,136,256]{2,1,0:T(8,128)(2,1)}), bf16[4,136,256]{2,1,0:T(8,128)(2,1)S(1)}, u32[]{:S(2)}, u32[]{:S(2)}) async-start(bf16[4,136,256]{2,1,0:T(8,128)(2,1)} %copy.86), calls=%async_computation.5 | async-start | bytes 557056 | tf_op jit(solution)/shard_map/all_to_all | solution.py:113
  126.4 3.0 %convolution_convert_fusion.1 = bf16[544,512]{1,0:T(8,128)(2,1)} fusion(bf16[544,1024]{0,1:T(8,128)(2,1)S(1)} %copy-done.5, bf16[512,2048]{1,0:T(8,128)(2,1)} %constant_dynamic-update-slice_fusion, s32[]{:T(128)S(6)} %select_n.19), kind=kOutput, calls=%fused_computation.16 | convolution fusion | flops 570703872 | bytes 2719748 | tf_op jit(solution)/shard_map/dot_general | solution.py:115
  129.4 3.6 %all-to-all-done.5 = bf16[4,136,256]{2,1,0:T(8,128)(2,1)S(1)} async-done(((bf16[4,136,256]{2,1,0:T(8,128)(2,1)}), bf16[4,136,256]{2,1,0:T(8,128)(2,1)S(1)}, u32[]{:S(2)}, u32[]{:S(2)}) %all-to-all-start.5) | async-done | bytes 278560 | tf_op jit(solution)/shard_map/all_to_all | solution.py:113
  133.0 3.5 %all-to-all-start.6 = ((bf16[4,136,512]{2,1,0:T(8,128)(2,1)}), bf16[4,136,512]{2,1,0:T(8,128)(2,1)S(1)}, u32[]{:S(2)}, u32[]{:S(2)}) async-start(bf16[4,136,512]{2,1,0:T(8,128)(2,1)} %bitcast.11), calls=%async_computation.6 | async-start | bytes 1114112 | tf_op jit(solution)/shard_map/all_to_all | solution.py:118
  138.5 11.0 %all-to-all-done.6 = bf16[4,136,512]{2,1,0:T(8,128)(2,1)S(1)} async-done(((bf16[4,136,512]{2,1,0:T(8,128)(2,1)}), bf16[4,136,512]{2,1,0:T(8,128)(2,1)S(1)}, u32[]{:S(2)}, u32[]{:S(2)}) %all-to-all-start.6) | async-done | bytes 557088 | tf_op jit(solution)/shard_map/all_to_all | solution.py:118
  150.9 3.2 %reduce-scatter.2.cloned.1.call-done = bf16[128,512]{1,0:T(8,128)(2,1)} async-done(((bf16[1024,512]{1,0:T(8,128)(2,1)}), bf16[128,512]{1,0:T(8,128)(2,1)}) %reduce-scatter.2.cloned.1.call-update) | async-done | bytes 131088 | tf_op jit(solution)/shard_map/reduce_scatter | solution.py:102
  (85 shorter events, 36.5 us)
Async XLA Ops:
  7.2 21.0 %copy-start.3 = (bf16[1,136,1024]{2,1,0:T(8,128)(2,1)S(1)}, bf16[1,136,1024]{2,1,0:T(8,128)(2,1)}, u32[]{:S(2)}) copy-start(bf16[1,136,1024]{2,1,0:T(8,128)(2,1)} %param.19) | copy-start | bytes 835588
  8.4 30.4 %copy-start.4 = (bf16[1,136,1024]{2,1,0:T(8,128)(2,1)S(1)}, bf16[1,136,1024]{2,1,0:T(8,128)(2,1)}, u32[]{:S(2)}) copy-start(bf16[1,136,1024]{2,1,0:T(8,128)(2,1)} %param.18) | copy-start | bytes 835588
  9.1 15.6 %all-to-all-start.1 = ((bf16[136,4,256]{2,0,1:T(8,128)(2,1)}), bf16[136,4,256]{2,0,1:T(8,128)(2,1)S(1)}, u32[]{:S(2)}, u32[]{:S(2)}) async-start(bf16[136,4,256]{2,0,1:T(8,128)(2,1)} %copy.62), calls=%async_computation.1 | async-start | bytes 557056 | tf_op jit(solution)/shard_map/all_to_all | solution.py:82
  16.6 32.5 %copy-start.1 = (bf16[512,128]{1,0:T(8,128)(2,1)S(1)}, bf16[512,128]{1,0:T(8,128)(2,1)}, u32[]{:S(2)}) copy-start(bf16[512,128]{1,0:T(8,128)(2,1)} %param.21) | copy-start | bytes 393220
  17.4 42.4 %copy-start = (bf16[1,136,2048]{2,1,0:T(8,128)(2,1)S(1)}, bf16[1,136,2048]{2,1,0:T(8,128)(2,1)}, u32[]{:S(2)}) copy-start(bf16[1,136,2048]{2,1,0:T(8,128)(2,1)} %param.15) | copy-start | bytes 1671172
  24.7 10.6 %all-to-all-start = ((bf16[136,4,256]{2,0,1:T(8,128)(2,1)}), bf16[136,4,256]{2,0,1:T(8,128)(2,1)S(1)}, u32[]{:S(2)}, u32[]{:S(2)}) async-start(bf16[136,4,256]{2,0,1:T(8,128)(2,1)} %copy.61), calls=%async_computation | async-start | bytes 557056 | tf_op jit(solution)/shard_map/all_to_all | solution.py:81
  35.3 10.3 %all-to-all-start.2 = ((bf16[136,4,256]{2,0,1:T(8,128)(2,1)}), bf16[136,4,256]{2,0,1:T(8,128)(2,1)S(1)}, u32[]{:S(2)}, u32[]{:S(2)}) async-start(bf16[136,4,256]{2,0,1:T(8,128)(2,1)} %copy.65), calls=%async_computation.2 | async-start | bytes 557056 | tf_op jit(solution)/shard_map/all_to_all | solution.py:84
  45.7 22.0 %all-to-all-start.3 = ((bf16[136,4,256]{2,0,1:T(8,128)(2,1)}), bf16[136,4,256]{2,0,1:T(8,128)(2,1)S(1)}, u32[]{:S(2)}, u32[]{:S(2)}) async-start(bf16[136,4,256]{2,0,1:T(8,128)(2,1)} %copy.66), calls=%async_computation.3 | async-start | bytes 557056 | tf_op jit(solution)/shard_map/all_to_all | solution.py:83
  49.1 5.3 %collective-permute-start = (bf16[512,128]{1,0:T(8,128)(2,1)S(1)}, bf16[512,128]{1,0:T(8,128)(2,1)S(1)}, u32[]{:S(2)}, u32[]{:S(2)}) collective-permute-start(bf16[512,128]{1,0:T(8,128)(2,1)S(1)} %copy-done.1), channel_id=1, source_target_pairs={{0,1},{1,2},{2,3},{3,4},{4,5},{5,6},{6,7},{7,0},{8,9},{9,10},{10,1... | collective-permute-start | bytes 393224 | tf_op jit(solution)/shard_map/ppermute | solution.py:19
  54.5 5.3 %collective-permute-start.1 = (bf16[512,128]{1,0:T(8,128)(2,1)S(1)}, bf16[512,128]{1,0:T(8,128)(2,1)S(1)}, u32[]{:S(2)}, u32[]{:S(2)}) collective-permute-start(bf16[512,128]{1,0:T(8,128)(2,1)S(1)} %collective-permute-done), channel_id=1, source_target_pairs={{0,1},{1,2},{2,3},{3,4},{4,5},{5,6},{6,7},{7,0},{8,9},{9,10},{10,1... | collective-permute-start | bytes 393224 | tf_op jit(solution)/shard_map/ppermute | solution.py:19
  59.8 5.3 %collective-permute-start.2 = (bf16[512,128]{1,0:T(8,128)(2,1)S(1)}, bf16[512,128]{1,0:T(8,128)(2,1)S(1)}, u32[]{:S(2)}, u32[]{:S(2)}) collective-permute-start(bf16[512,128]{1,0:T(8,128)(2,1)S(1)} %collective-permute-done.1), channel_id=1, source_target_pairs={{0,1},{1,2},{2,3},{3,4},{4,5},{5,6},{6,7},{7,0},{8,9},{9,10},{10,1... | collective-permute-start | bytes 393224 | tf_op jit(solution)/shard_map/ppermute | solution.py:19
  65.1 19.8 %collective-permute-start.3 = (bf16[512,128]{1,0:T(8,128)(2,1)S(1)}, bf16[512,128]{1,0:T(8,128)(2,1)S(1)}, u32[]{:S(2)}, u32[]{:S(2)}) collective-permute-start(bf16[512,128]{1,0:T(8,128)(2,1)S(1)} %collective-permute-done.2), channel_id=1, source_target_pairs={{0,1},{1,2},{2,3},{3,4},{4,5},{5,6},{6,7},{7,0},{8,9},{9,10},{10,1... | collective-permute-start | bytes 393224 | tf_op jit(solution)/shard_map/ppermute | solution.py:19
  66.0 7.0 %copy-start.6 = (f32[1,4,544]{2,1,0:T(4,128)S(1)}, f32[1,4,544]{2,1,0:T(4,128)}, u32[]{:S(2)}) copy-start(f32[1,4,544]{2,1,0:T(4,128)} %param.20) | copy-start | bytes 26116
  67.7 40.6 %all-to-all-start.7 = ((bf16[136,4,512]{2,0,1:T(8,128)(2,1)}), bf16[136,4,512]{2,0,1:T(8,128)(2,1)S(1)}, u32[]{:S(2)}, u32[]{:S(2)}) async-start(bf16[136,4,512]{2,0,1:T(8,128)(2,1)} %copy.80), calls=%async_computation.7 | async-start | bytes 1114112 | tf_op jit(solution)/shard_map/all_to_all | solution.py:85
  72.7 43.4 %all-gather.2.cloned.1.call-start = ((), (), s32[]{:S(2)}) async-start(), calls=%async_computation.9 | async-start | bytes 1638400 | tf_op jit(solution)/shard_map/all_gather | solution.py:100
  73.0 4.3 %copy-start.2 = (bf16[544,4,64]{0,2,1:T(8,128)(2,1)S(1)}, bf16[544,4,64]{0,2,1:T(8,128)(2,1)}, u32[]{:S(2)}) copy-start(bf16[544,4,64]{0,2,1:T(8,128)(2,1)} %copy.67) | copy-start | bytes 835588
  84.8 5.3 %collective-permute-start.4 = (bf16[512,128]{1,0:T(8,128)(2,1)S(1)}, bf16[512,128]{1,0:T(8,128)(2,1)S(1)}, u32[]{:S(2)}, u32[]{:S(2)}) collective-permute-start(bf16[512,128]{1,0:T(8,128)(2,1)S(1)} %collective-permute-done.3), channel_id=1, source_target_pairs={{0,1},{1,2},{2,3},{3,4},{4,5},{5,6},{6,7},{7,0},{8,9},{9,10},{10,1... | collective-permute-start | bytes 393224 | tf_op jit(solution)/shard_map/ppermute | solution.py:19
  90.2 5.3 %collective-permute-start.5 = (bf16[512,128]{1,0:T(8,128)(2,1)S(1)}, bf16[512,128]{1,0:T(8,128)(2,1)S(1)}, u32[]{:S(2)}, u32[]{:S(2)}) collective-permute-start(bf16[512,128]{1,0:T(8,128)(2,1)S(1)} %collective-permute-done.4), channel_id=1, source_target_pairs={{0,1},{1,2},{2,3},{3,4},{4,5},{5,6},{6,7},{7,0},{8,9},{9,10},{10,1... | collective-permute-start | bytes 393224 | tf_op jit(solution)/shard_map/ppermute | solution.py:19
  95.5 5.3 %collective-permute-start.6 = (bf16[512,128]{1,0:T(8,128)(2,1)S(1)}, bf16[512,128]{1,0:T(8,128)(2,1)S(1)}, u32[]{:S(2)}, u32[]{:S(2)}) collective-permute-start(bf16[512,128]{1,0:T(8,128)(2,1)S(1)} %collective-permute-done.5), channel_id=1, source_target_pairs={{0,1},{1,2},{2,3},{3,4},{4,5},{5,6},{6,7},{7,0},{8,9},{9,10},{10,1... | collective-permute-start | bytes 393224 | tf_op jit(solution)/shard_map/ppermute | solution.py:19
  108.3 13.3 %all-to-all-start.4 = ((bf16[4,136,256]{2,1,0:T(8,128)(2,1)}), bf16[4,136,256]{2,1,0:T(8,128)(2,1)S(1)}, u32[]{:S(2)}, u32[]{:S(2)}) async-start(bf16[4,136,256]{2,1,0:T(8,128)(2,1)} %copy.85), calls=%async_computation.4 | async-start | bytes 557056 | tf_op jit(solution)/shard_map/all_to_all | solution.py:112
  113.4 40.7 %reduce-scatter.2.cloned.1.call-start = ((), (), s32[]{:S(2)}) async-start(), calls=%async_computation.10 | async-start | bytes 1179648 | tf_op jit(solution)/shard_map/reduce_scatter | solution.py:102
  119.4 6.9 %copy-start.5 = (bf16[544,1024]{0,1:T(8,128)(2,1)S(1)}, bf16[544,1024]{0,1:T(8,128)(2,1)}, u32[]{:S(2)}) copy-start(bf16[544,1024]{0,1:T(8,128)(2,1)} %all-gather.2.cloned.1.call-done) | copy-start | bytes 3342340
  121.5 11.4 %all-to-all-start.5 = ((bf16[4,136,256]{2,1,0:T(8,128)(2,1)}), bf16[4,136,256]{2,1,0:T(8,128)(2,1)S(1)}, u32[]{:S(2)}, u32[]{:S(2)}) async-start(bf16[4,136,256]{2,1,0:T(8,128)(2,1)} %copy.86), calls=%async_computation.5 | async-start | bytes 557056 | tf_op jit(solution)/shard_map/all_to_all | solution.py:113
  133.0 16.5 %all-to-all-start.6 = ((bf16[4,136,512]{2,1,0:T(8,128)(2,1)}), bf16[4,136,512]{2,1,0:T(8,128)(2,1)S(1)}, u32[]{:S(2)}, u32[]{:S(2)}) async-start(bf16[4,136,512]{2,1,0:T(8,128)(2,1)} %bitcast.11), calls=%async_computation.6 | async-start | bytes 1114112 | tf_op jit(solution)/shard_map/all_to_all | solution.py:118
  (2 other events, 8.1 us)
Sparse Core Ops, SparseCore 0:
  81.3 34.8 all-gather.1
  119.6 34.4 reduce-scatter.1
